TPU v7x, 32 devices: a whole 2x2x4 slice. The times are simulated.
32 devices in a mesh: sp: 8 (over z, y), tp: 4 (over x, core).
Axes of the slice: x: 2, y: 2, z: 4, core: 2. Of those that a mesh axis runs over, the one named last changes fastest.
Arguments:
- tokens: bfloat16 [4, 1024, 2048], P(None, 'sp'), may hold values from -6 to 6
- next_tokens: bfloat16 [4, 2048], replicated, may hold values from -6 to 6
- w_query: bfloat16 [2048, 2048], P(None, 'tp'), may hold values from -0.125 to 0.125
- w_key: bfloat16 [2048, 2048], P(None, 'tp'), may hold values from -0.125 to 0.125
- w_value: bfloat16 [2048, 2048], P(None, 'tp'), may hold values from -0.125 to 0.125
- w_in_gate: bfloat16 [2048, 8], replicated, may hold values from -0.125 to 0.125
- w_forget_gate: bfloat16 [2048, 8], replicated, may hold values from -0.125 to 0.125
- forget_bias: float32 [8], replicated, may hold values from 3 to 14
- extra_decay: float32 [8, 4, 1024], P('tp', None, 'sp'), may hold values from -0.5509766 to 0
- w_out: bfloat16 [2048, 2048], P('tp'), may hold values from -0.125 to 0.125
Outputs:
- memory: bfloat16 [8, 1024, 256], P('tp', 'sp')
- normalizer: float32 [8, 1024], P('tp', 'sp')
- stabilizer: float32 [4, 8], P(None, 'tp')
- read: bfloat16 [4, 2048], replicated
All inputs are finite; a program needn't handle non-finite values.
Results may differ from a plain program's by a relative error of at most 0.024.
Values may be sent and summed in bfloat16 or wider, within the bound.
A program may use at most 64 MiB of HBM per device.

v0:
```python
import jax
import jax.numpy as jnp
from jax import lax
from jax.sharding import PartitionSpec as P

HD = 256


def per_device(
    tokens,
    next_tokens,
    w_query,
    w_key,
    w_value,
    w_in_gate,
    w_forget_gate,
    forget_bias,
    extra_decay,
    w_out,
):
    scale = HD ** (-0.5)
    seq_count = tokens.shape[0]
    span = tokens.shape[1]
    heads_here = w_key.shape[1] // HD
    sp_size = lax.axis_size("sp")
    sp_index = lax.axis_index("sp")
    head_start = lax.axis_index("tp") * heads_here
    gate_in = lax.dynamic_slice_in_dim(w_in_gate, head_start, heads_here, 1)
    gate_forget = lax.dynamic_slice_in_dim(w_forget_gate, head_start, heads_here, 1)
    bias_here = lax.dynamic_slice_in_dim(forget_bias, head_start, heads_here, 0)
    flat = tokens.reshape(seq_count * span, tokens.shape[2])
    keys = jnp.dot(flat, w_key, preferred_element_type=jnp.float32).astype(jnp.bfloat16)
    values = jnp.dot(flat, w_value, preferred_element_type=jnp.float32).astype(jnp.bfloat16)
    log_in = jnp.dot(flat, gate_in, preferred_element_type=jnp.float32).reshape(
        seq_count, span, heads_here
    )
    log_forget = jax.nn.log_sigmoid(
        jnp.dot(flat, gate_forget, preferred_element_type=jnp.float32) + bias_here
    ).reshape(seq_count, span, heads_here) + jnp.transpose(extra_decay, (1, 2, 0))
    prefix = jnp.cumsum(log_forget, axis=1)
    block_total = prefix[:, -1]
    local_score = block_total[:, None, :] - prefix + log_in
    block_peak = jnp.max(local_score, axis=1)
    totals, peaks = (
        lax.all_gather(block_total[None], "sp", axis=0, tiled=True),
        lax.all_gather(block_peak[None], "sp", axis=0, tiled=True),
    )
    later = jnp.flip(jnp.cumsum(jnp.flip(totals, 0), axis=0), 0) - totals
    prompt_total = jnp.sum(totals, axis=0)
    stabilizer = jnp.maximum(prompt_total, jnp.max(later + peaks, axis=0))
    pick_block = (jnp.arange(sp_size) == sp_index).astype(jnp.float32)
    later_here = jnp.sum(pick_block[:, None, None] * later, axis=0)
    weight = jnp.exp(later_here[:, None, :] + local_score - stabilizer[:, None, :]) * scale
    key_heads = keys.reshape(seq_count, span, heads_here, HD)
    value_heads = values.reshape(seq_count, span, heads_here, HD)
    weighted = (key_heads.astype(jnp.float32) * weight[:, :, :, None]).astype(jnp.bfloat16)
    block_memory = jnp.einsum(
        "sthd,sthe->hsde", weighted, value_heads, preferred_element_type=jnp.float32
    )
    block_norm = jnp.transpose(jnp.sum(weighted.astype(jnp.float32), axis=1), (1, 0, 2))
    memory_term = block_memory.reshape(heads_here, seq_count * HD, HD)
    norm_term = block_norm.reshape(heads_here, seq_count * HD)
    memory_rows, norm_rows = (
        lax.psum_scatter(memory_term, "sp", scatter_dimension=1, tiled=True),
        lax.psum_scatter(norm_term, "sp", scatter_dimension=1, tiled=True),
    )
    query = (
        jnp.dot(next_tokens, w_query, preferred_element_type=jnp.float32)
        .astype(jnp.bfloat16)
        .astype(jnp.float32)
        .reshape(seq_count, heads_here, HD)
    )
    new_key = (
        jnp.dot(next_tokens, w_key, preferred_element_type=jnp.float32)
        .astype(jnp.bfloat16)
        .astype(jnp.float32)
        .reshape(seq_count, heads_here, HD)
        * scale
    )
    new_value = (
        jnp.dot(next_tokens, w_value, preferred_element_type=jnp.float32)
        .astype(jnp.bfloat16)
        .astype(jnp.float32)
        .reshape(seq_count, heads_here, HD)
    )
    new_in = jnp.dot(next_tokens, gate_in, preferred_element_type=jnp.float32)
    new_forget = jax.nn.log_sigmoid(
        jnp.dot(next_tokens, gate_forget, preferred_element_type=jnp.float32) + bias_here
    )
    numer_slots = jnp.einsum("shd,hsde->she", query, block_memory, precision=lax.Precision.HIGHEST)
    denom_slots = jnp.einsum("shd,hsd->sh", query, block_norm, precision=lax.Precision.HIGHEST)
    query_state, query_norm = lax.psum((numer_slots, denom_slots), "sp")
    top = jnp.maximum(new_forget + stabilizer, new_in)
    keep = jnp.exp(new_forget + stabilizer - top)
    take = jnp.exp(new_in - top)
    qk = jnp.sum(query * new_key, axis=-1)
    numer = keep[:, :, None] * query_state + (take * qk)[:, :, None] * new_value
    denom = keep * query_norm + take * qk
    head_out = (numer / jnp.maximum(jnp.abs(denom), 1.0)[:, :, None]).astype(jnp.bfloat16)
    partial_value = (
        jnp.dot(
            head_out.reshape(seq_count, heads_here * HD), w_out, preferred_element_type=jnp.float32
        )
        .astype(jnp.bfloat16)
        .astype(jnp.float32)
    )
    read = lax.psum(partial_value.astype(jnp.bfloat16), "tp")
    return (memory_rows.astype(jnp.bfloat16), norm_rows, stabilizer, read)


def solution(mesh):
    placed = (
        P(None, "sp", None),
        P(),
        P(None, "tp"),
        P(None, "tp"),
        P(None, "tp"),
        P(),
        P(),
        P(),
        P("tp", None, "sp"),
        P("tp", None),
    )
    return jax.shard_map(
        per_device,
        mesh=mesh,
        in_specs=placed,
        out_specs=(P("tp", "sp", None), P("tp", "sp"), P(None, "tp"), P()),
        check_vma=False,
    )
```

profile of v0, /device:TPU:0, one launch (start us, length us, event | category | flops | bytes accessed | tf_op | source)
XLA Modules:
  0.0 210.3 jit_solution(8536744384994718266)
XLA Ops:
  7.2 0.0 reduce-scatter.7.cloned.1.call-start
  7.2 0.9 dynamic_slice.10
  8.1 0.7 copy-done
  8.8 1.4 fusion.16
  10.3 0.1 copy.40
  10.4 0.3 reduce_window_sum.22
  10.7 27.9 %all-gather = f32[32,1,2]{2,1,0:T(1,128)S(1)} all-gather(f32[4,1,2]{2,1,0:T(1,128)S(1)} %slice.4), channel_id=2, replica_groups=mesh['sp'=8,'tp'=4] {'sp'}, dimensions={0}, use_global_device_ids=true | all-gather | bytes 288 | tf_op jit(solution)/shard_map/all_gather | solution.py:45
  38.6 0.1 copy.63
  38.8 2.8 %fusion.2 = f32[512,512]{1,0:T(8,128)S(1)} fusion(bf16[512,2048]{1,0:T(8,128)(2,1)S(1)} %bitcast.53, bf16[2048,512]{1,0:T(8,128)(2,1)} %param.13), kind=kOutput, calls=%fused_computation.5 | convolution fusion | flops 1074266112 | bytes 5242880 | tf_op jit(solution)/shard_map/dot_general | solution.py:32
  41.6 1.6 reshape.82
  43.3 1.5 copy.50
  44.7 0.1 copy.69
  44.9 0.6 convolution_bitcast_fusion
  45.5 0.9 copy.65
  46.4 1.0 fusion.13
  47.4 0.1 copy.46
  47.5 19.0 %all-gather.2 = f32[8,4,2]{1,2,0:T(2,128)S(1)} all-gather(f32[1,4,2]{1,2,0:T(2,128)S(1)} %bitcast.68), channel_id=3, replica_groups=mesh['sp'=8,'tp'=4] {'sp'}, dimensions={0}, use_global_device_ids=true | all-gather | bytes 288 | tf_op jit(solution)/shard_map/all_gather | solution.py:46
  66.5 0.1 multiply_reduce_fusion.1
  66.6 0.1 copy.48
  66.7 0.1 copy.42
  66.8 1.7 exponential_multiply_fusion
  68.5 1.1 copy.49
  69.5 0.4 convert_reduce_fusion
  69.9 1.0 copy.68
  71.0 0.0 reduce-scatter.5.cloned.1.call-start
  71.0 3.6 %convolution_convert_fusion.1 = bf16[512,512]{1,0:T(8,128)(2,1)} fusion(bf16[512,2048]{1,0:T(8,128)(2,1)S(1)} %bitcast.56, bf16[2048,512]{1,0:T(8,128)(2,1)} %param.14), kind=kOutput, calls=%fused_computation.3 | convolution fusion | flops 1074003968 | bytes 4718592 | tf_op jit(solution)/shard_map/dot_general | solution.py:33
  74.6 2.0 reshape.75
  76.6 2.8 %fusion.11 = f32[2,4,256,256]{3,2,1,0:T(8,128)} fusion(bf16[4,128,2,256]{3,2,1,0:T(2,128)(2,1)} %reshape.75, f32[4,128,2,256]{1,3,0,2:T(8,128)S(1)} %copy.50, f32[4,128,2]{1,0,2:T(4,128)S(1)} %copy.49), kind=kOutput, calls=%fused_computation.23 | convolution fusion | flops 134742016 | bytes 3674112 | tf_op jit(solution)/shard_map/sthd,sthe->hsde/dot_general | solution.py:57
  79.5 2.0 convolution_convert_fusion.5
  81.5 2.4 %fusion = f32[4,2,1,256]{3,2,1,0:T(1,128)S(1)} fusion(bf16[4,2,256,1]{2,3,1,0:T(2,128)(2,1)S(1)} %reshape.95, f32[2,4,256,256]{3,2,1,0:T(8,128)} %fusion.11), kind=kOutput, calls=%fused_computation.1 | convolution fusion | flops 6291456 | bytes 2109440 | tf_op jit(solution)/shard_map/shd,hsde->she/dot_general | solution.py:90
  83.9 0.1 multiply_reduce_fusion
  84.0 17.7 %all-reduce = (f32[4,2]{0,1:T(2,128)S(1)}, f32[4,2,256]{2,1,0:T(2,128)S(1)}) all-reduce(f32[4,2]{0,1:T(2,128)S(1)} %multiply_reduce_fusion, f32[4,2,256]{2,1,0:T(2,128)S(1)} %bitcast.66), channel_id=1, replica_groups=mesh['sp'=8,'tp'=4] {'sp'}, use_global_device_ids=true, to_apply=%region_11.12 | all-reduce | flops 2056 | bytes 16448 | tf_op jit(solution)/shard_map/psum | solution.py:92
  101.7 2.0 fusion.6
  103.7 0.1 reduce_sum.39
  103.8 0.1 copy.53
  103.9 0.1 convolution_bitcast_fusion.1
  104.0 0.9 abs_maximum_fusion
  104.9 0.1 copy.55
  105.0 2.0 fusion.3
  107.1 0.1 copy.54
  107.1 0.1 copy.52
  107.2 0.1 fusion.17
  107.3 2.0 convolution_convert_fusion
  109.3 10.7 %psum.23 = bf16[4,2048]{1,0:T(4,128)(2,1)} all-reduce(bf16[4,2048]{1,0:T(4,128)(2,1)S(1)} %convolution_convert_fusion), channel_id=1, replica_groups=mesh['sp'=8,'tp'=4] {'tp'}, use_global_device_ids=true, to_apply=%region_12.13 | all-reduce | flops 8192 | bytes 32768 | tf_op jit(solution)/shard_map/psum | solution.py:107
  120.0 11.0 %reduce-scatter.7.cloned.1.call-done = f32[128,2]{1,0:T(8,128)} async-done(((f32[1024,2]{1,0:T(8,128)}), f32[128,2]{1,0:T(8,128)}) %reduce-scatter.7.cloned.1.call-update) | async-done | bytes 1040
  131.0 1.5 copy.67
  132.5 69.4 %reduce-scatter.5.cloned.1.call-done = f32[2,128,256]{2,1,0:T(8,128)} async-done(((f32[2,1024,256]{2,1,0:T(8,128)}), f32[2,128,256]{2,1,0:T(8,128)}) %reduce-scatter.5.cloned.1.call-update) | async-done | bytes 262160 | tf_op jit(solution)/shard_map/reduce_scatter | solution.py:64
  201.9 1.6 convert_element_type.58
  (27 shorter events, 0.2 us)
Async XLA Ops:
  7.2 1.6 copy-start
  7.2 3.1 %copy-start.2 = (f32[2,4,128]{2,1,0:T(4,128)S(1)}, f32[2,4,128]{2,1,0:T(4,128)}, u32[]{:S(2)}) copy-start(f32[2,4,128]{2,1,0:T(4,128)} %param.18) | copy-start | bytes 12292
  7.2 123.8 %reduce-scatter.7.cloned.1.call-start = ((), (), s32[]{:S(2)}) async-start(), calls=%async_computation.3 | async-start | bytes 589824
  41.6 3.3 %copy-start.4 = (bf16[2048,8]{0,1:T(8,128)(2,1)S(1)}, bf16[2048,8]{0,1:T(8,128)(2,1)}, u32[]{:S(2)}) copy-start(bf16[2048,8]{0,1:T(8,128)(2,1)} %param.15) | copy-start | bytes 98308
  66.6 37.5 %copy-start.3 = (f32[4,2]{0,1:T(2,128)}, f32[4,2]{0,1:T(2,128)S(1)}, u32[]{:S(2)}) copy-start(f32[4,2]{0,1:T(2,128)S(1)} %max.30) | copy-start | bytes 100
  71.0 130.9 %reduce-scatter.5.cloned.1.call-start = ((), (), s32[]{:S(2)}) async-start(), calls=%async_computation.2 | async-start | bytes 2359296 | tf_op jit(solution)/shard_map/reduce_scatter | solution.py:64
  76.6 2.9 %copy-start.1 = (bf16[4,2048]{1,0:T(4,128)(2,1)S(1)}, bf16[4,2048]{1,0:T(4,128)(2,1)}, u32[]{:S(2)}) copy-start(bf16[4,2048]{1,0:T(4,128)(2,1)} %param.11) | copy-start | bytes 49156
Sparse Core Ops, SparseCore 0:
  71.1 59.8 reduce-scatter.6
  134.5 67.3 reduce-scatter.4
where the time goes:
time: 211 us; the launch traced here: 210 us
  waiting for transfers between devices  80.4 us (38%)
  blocking collectives  75.4 us (36%)
  matrix products  22.7 us (11%)
  between operations  14.2 us (7%)
  local copies, waits for them, and re-layouts  12.2 us (6%)
  other arithmetic  5.39 us (3%)
    reduce_scatter x1, waiting for transfers between devices, per_device(): lax.psum_scatter(memory_term, 'sp', scatter_dimension=1, tiled=True)  69.4 us
    all_gather x1, blocking collectives, per_device(): lax.all_gather(block_total[None], 'sp', axis=0, tiled=True)  27.9 us
    all_gather x1, blocking collectives, per_device(): lax.all_gather(block_peak[None], 'sp', axis=0, tiled=True)  19 us
    psum x1, blocking collectives, per_device(): query_state, query_norm = lax.psum((numer_slots, denom_slots), 'sp')  17.7 us
    unnamed x3, waiting for transfers between devices  11 us
    psum x1, blocking collectives, per_device(): read = lax.psum(partial_value.astype(jnp.bfloat16), 'tp')  10.7 us
  transfers between devices with their start and end apart: 2, of which 2 were waited for; matrix products, arithmetic and copies ran while one was open for 10% of the time, Pallas kernels for 0%

commit v1 on v0

v1 whole, which is shorter than its diff:
```python
import functools

import jax
import jax.numpy as jnp
from jax import lax
from jax.experimental import pallas as pl
from jax.experimental.pallas import tpu as pltpu
from jax.sharding import PartitionSpec as P

HD = 256
LANES = 128
F32 = jnp.float32
BF16 = jnp.bfloat16
HIGHEST = lax.Precision.HIGHEST


def log_sigmoid(x):
    return jnp.minimum(x, 0.0) - jnp.log1p(jnp.exp(-jnp.abs(x)))


def dot(a, b, dims=((1,), (0,)), precision=None):
    return lax.dot_general(a, b, (dims, ((), ())), precision=precision, preferred_element_type=F32)


def kernel(
    seqs, span, heads, sp, tp,
    tokens, next_tokens, w_query, w_key, w_value, w_in, w_forget, bias, decay, w_out,
    mem_out, norm_out, stab_out, read_out,
    x, wq, wk, wv, wo, wg, bias_wide, decay_wide, stats, state, pair_send, pair_recv,
    far_send, far_recv, slots, parts,
    load_sem, stat_ss, stat_rs, pair_ss, pair_rs, far_ss, far_rs, slot_ss, slot_rs, part_ss, part_rs,
):
    me = lax.axis_index("sp")
    me_tp = lax.axis_index("tp")
    count = seqs * span
    rows = seqs * HD // sp
    groups = sp // 2
    group = me // 2
    side = lax.rem(me, 2)
    partner = me + 1 - 2 * side
    scale = HD ** (-0.5)

    loads = []

    def load(src, dst):
        loads.append(pltpu.make_async_copy(src, dst, load_sem.at[len(loads)]))
        loads[-1].start()
        return loads[-1]

    load_x = load(tokens, x.at[pl.ds(0, count)])
    load_k = [None] * heads
    load_v = [None] * heads
    for h in range(heads):
        cols = pl.ds(h * HD, HD)
        load_k[h] = load(w_key.at[:, cols], wk.at[h])
        load_v[h] = load(w_value.at[:, cols], wv.at[h])
    load_q = load(w_query, wq)
    load_o = load(w_out, wo)

    barrier = pltpu.get_barrier_semaphore()
    for k in range(1, sp):
        pl.semaphore_signal(barrier, inc=1, device_id={"sp": lax.rem(me + k, sp)})
    for k in range(1, tp):
        pl.semaphore_signal(barrier, inc=1, device_id={"tp": lax.rem(me_tp + k, tp)})

    def send(src, dst, ss, rs, where):
        copy = pltpu.make_async_remote_copy(
            src_ref=src, dst_ref=dst, send_sem=ss, recv_sem=rs, device_id=where
        )
        copy.start()
        return copy

    x[pl.ds(count, 16), :] = jnp.zeros((16, x.shape[1]), BF16)
    x[pl.ds(count, seqs), :] = next_tokens[...]
    wg[...] = jnp.zeros_like(wg)
    width = w_in.shape[1]
    wg[:, 0:width] = w_in[...]
    wg[:, LANES : LANES + width] = w_forget[...]
    bias_wide[...] = jnp.zeros_like(bias_wide)
    bias_wide[0:1, 0:width] = bias[...]
    decay_wide[...] = jnp.zeros_like(decay_wide)
    for p in range(seqs):
        for h in range(heads):
            decay_wide[p, h : h + 1, :] = decay[h, p : p + 1, :]

    load_x.wait()
    gates = dot(x[...], wg[...])
    shift = lax.rem(LANES - me_tp * heads, LANES)
    log_in = pltpu.roll(gates[:, :LANES], shift, 1)
    forget = pltpu.roll(log_sigmoid(gates[:, LANES:] + bias_wide[0:1, :]), shift, 1)
    after = (
        lax.broadcasted_iota(jnp.int32, (span, span), 1)
        > lax.broadcasted_iota(jnp.int32, (span, span), 0)
    ).astype(F32)
    weight = []
    for p in range(seqs):
        block = forget[p * span : (p + 1) * span] + decay_wide[p].T
        score = dot(after, block, precision=HIGHEST) + log_in[p * span : (p + 1) * span]
        peak = jnp.max(score, axis=0, keepdims=True)
        stats[0, p : p + 1, :] = jnp.sum(block, axis=0, keepdims=True)
        stats[0, seqs + p : seqs + p + 1, :] = peak
        weight.append(jnp.exp(score - peak) * scale)
    weight = jnp.concatenate(weight, axis=0)
    new_in = log_in[count : count + seqs]
    new_forget = forget[count : count + seqs]

    pl.semaphore_wait(barrier, sp - 1 + tp - 1)
    stat_copies = [
        send(stats.at[0], stats.at[k], stat_ss.at[k], stat_rs.at[k], {"sp": lax.rem(me + k, sp)})
        for k in range(1, sp)
    ]

    order = list(range(1, groups)) + [0]
    if groups > 2:
        order = [groups // 2] + [k for k in order if k != groups // 2]
    mask = (
        lax.broadcasted_iota(jnp.int32, (16, count), 1) // span
        == lax.broadcasted_iota(jnp.int32, (16, count), 0)
    )
    pick = jnp.where(mask, 1.0, 0.0).astype(BF16)
    factor = None
    query = None
    pair_copies = {}
    new_keys, new_values, queries = [], [], []
    slot_copies = []

    for h in range(heads):
        load_k[h].wait()
        keys = dot(x[...], wk[h]).astype(BF16)
        load_v[h].wait()
        values = dot(x[...], wv[h]).astype(BF16)
        weighted = (keys[:count].astype(F32) * weight[:, h : h + 1]).astype(BF16)
        new_keys.append(keys[count : count + seqs].astype(F32) * scale)
        new_values.append(values[count : count + seqs].astype(F32))
        if factor is None:
            for copy in stat_copies:
                copy.wait()
            later = jnp.zeros((seqs, LANES), F32)
            stab = None
            here = later
            for s in range(sp - 1, -1, -1):
                slot = lax.rem(me - s + sp, sp)
                peak = stats[slot, seqs : 2 * seqs, :]
                total = stats[slot, 0:seqs, :]
                stab = later + peak if stab is None else jnp.maximum(stab, later + peak)
                here = jnp.where(me == s, later + peak, here)
                later = later + total
            stab = jnp.maximum(stab, later)
            factor = jnp.exp(here - stab)
            stab_out[...] = stab
        for p in range(seqs):
            part = slice(p * span, (p + 1) * span)
            block = dot(weighted[part], values[part], ((0,), (0,)))
            state[h, pl.ds(p * HD, HD), :] = block * factor[p : p + 1, h : h + 1]
        for k in order:
            owner = 2 * lax.rem(group + k, groups) + 1 - side
            start = pl.multiple_of(owner * rows, rows)
            pair_send[h, k] = state[h, pl.ds(start, rows), :].astype(BF16)
            i = h * groups + k
            pair_copies[h, k] = send(
                pair_send.at[h, k], pair_recv.at[h, k], pair_ss.at[i], pair_rs.at[i],
                {"sp": partner},
            )
        if query is None:
            load_q.wait()
            query = dot(x[pl.ds(count, 16), :], wq[...]).astype(BF16)
        q = query[:, h * HD : (h + 1) * HD]
        queries.append(q[:seqs].astype(F32))
        reach = jnp.where(mask, dot(q, weighted, ((1,), (1,))), 0.0)
        high = reach.astype(BF16)
        low = (reach - high.astype(F32)).astype(BF16)
        product = dot(high, values[:count]) + dot(low, values[:count])
        norm = dot(pick, weighted)
        slots[0, 0, h] = product[:seqs] * factor[:, h : h + 1]
        slots[0, 1, h] = norm[:seqs] * factor[:, h : h + 1]

    slot_copies = [
        send(slots.at[0], slots.at[k], slot_ss.at[k], slot_rs.at[k], {"sp": lax.rem(me + k, sp)})
        for k in range(1, sp)
    ]

    far_copies = {}

    def forward(h):
        for k in order:
            pair_copies[h, k].wait()
            if k == 0:
                continue
            to = lax.rem(group + k, groups)
            start = pl.multiple_of((2 * to + side) * rows, rows)
            far_send[h, k] = (
                state[h, pl.ds(start, rows), :] + pair_recv[h, k].astype(F32)
            ).astype(BF16)
            i = h * groups + k
            far_copies[h, k] = send(
                far_send.at[h, k], far_recv.at[h, k], far_ss.at[i], far_rs.at[i],
                {"sp": 2 * to + side},
            )

    forward(0)

    for copy in slot_copies:
        copy.wait()
    total = [[None] * heads for _ in range(2)]
    for s in range(sp):
        slot = lax.rem(me - s + sp, sp)
        for kind in range(2):
            for h in range(heads):
                term = slots[slot, kind, h]
                total[kind][h] = term if s == 0 else total[kind][h] + term
    top = jnp.maximum(new_forget + stab, new_in)
    keep = jnp.exp(new_forget + stab - top)
    take = jnp.exp(new_in - top)
    outs = []
    for h in range(heads):
        norm_out[h] = total[1][h]
        keep_h = keep[:, h : h + 1]
        taken = take[:, h : h + 1] * jnp.sum(queries[h] * new_keys[h], axis=1, keepdims=True)
        numer = keep_h * total[0][h] + taken * new_values[h]
        denom = keep_h * jnp.sum(queries[h] * total[1][h], axis=1, keepdims=True) + taken
        outs.append(numer / jnp.maximum(jnp.abs(denom), 1.0))
    load_o.wait()
    outs = jnp.concatenate(outs, axis=1) if heads > 1 else outs[0]
    parts[0] = dot(outs.astype(BF16), wo[...]).astype(BF16)
    part_copies = [
        send(
            parts.at[0], parts.at[k], part_ss.at[k], part_rs.at[k],
            {"tp": lax.rem(me_tp + k, tp)},
        )
        for k in range(1, tp)
    ]
    for h in range(1, heads):
        forward(h)
    for copy in part_copies:
        copy.wait()
    read = None
    for t in range(tp):
        term = parts[lax.rem(me_tp - t + tp, tp)].astype(F32)
        read = term if read is None else read + term
    read_out[...] = read.astype(BF16)

    start = pl.multiple_of(me * rows, rows)
    for h in range(heads):
        mine = state[h, pl.ds(start, rows), :] + pair_recv[h, 0].astype(F32)
        for k in order[:-1]:
            far_copies[h, k].wait()
            mine = mine + far_recv[h, k].astype(F32)
        mem_out[h] = mine.astype(BF16)


def per_device(
    sp, tp,
    tokens, next_tokens, w_query, w_key, w_value, w_in_gate, w_forget_gate, forget_bias,
    extra_decay, w_out,
):
    seqs, span, model = tokens.shape
    heads = w_key.shape[1] // HD
    rows = seqs * HD // sp
    groups = sp // 2
    count = seqs * span
    any_spec = pl.BlockSpec(memory_space=pl.ANY)
    vmem = pl.BlockSpec(memory_space=pltpu.VMEM)
    dma = pltpu.SemaphoreType.DMA
    memory, norm, stab, read = pl.pallas_call(
        functools.partial(kernel, seqs, span, heads, sp, tp),
        out_shape=(
            jax.ShapeDtypeStruct((heads, rows, HD), BF16),
            jax.ShapeDtypeStruct((heads, seqs, HD), F32),
            jax.ShapeDtypeStruct((seqs, LANES), F32),
            jax.ShapeDtypeStruct((seqs, w_out.shape[1]), BF16),
        ),
        in_specs=[any_spec, vmem, any_spec, any_spec, any_spec, vmem, vmem, vmem, vmem, any_spec],
        out_specs=(vmem, vmem, vmem, vmem),
        scratch_shapes=[
            pltpu.VMEM((count + 16, model), BF16),
            pltpu.VMEM(w_query.shape, BF16),
            pltpu.VMEM((heads, model, HD), BF16),
            pltpu.VMEM((heads, model, HD), BF16),
            pltpu.VMEM(w_out.shape, BF16),
            pltpu.VMEM((model, 2 * LANES), BF16),
            pltpu.VMEM((8, LANES), F32),
            pltpu.VMEM((seqs, LANES, span), F32),
            pltpu.VMEM((sp, 2 * seqs, LANES), F32),
            pltpu.VMEM((heads, seqs * HD, HD), F32),
            pltpu.VMEM((heads, groups, rows, HD), BF16),
            pltpu.VMEM((heads, groups, rows, HD), BF16),
            pltpu.VMEM((heads, groups, rows, HD), BF16),
            pltpu.VMEM((heads, groups, rows, HD), BF16),
            pltpu.VMEM((sp, 2, heads, seqs, HD), F32),
            pltpu.VMEM((tp, seqs, w_out.shape[1]), BF16),
            dma((3 + 2 * heads,)),
            dma((sp,)),
            dma((sp,)),
            dma((heads * groups,)),
            dma((heads * groups,)),
            dma((heads * groups,)),
            dma((heads * groups,)),
            dma((sp,)),
            dma((sp,)),
            dma((tp,)),
            dma((tp,)),
        ],
        compiler_params=pltpu.CompilerParams(
            collective_id=0, has_side_effects=True, vmem_limit_bytes=56 * 1024 * 1024
        ),
    )(
        tokens.reshape(count, model), next_tokens, w_query, w_key, w_value, w_in_gate,
        w_forget_gate, forget_bias.reshape(1, -1), extra_decay, w_out,
    )
    start = lax.axis_index("sp") * rows
    norm_rows = lax.dynamic_slice_in_dim(norm.reshape(heads, seqs * HD), start, rows, 1)
    return memory, norm_rows, stab[:, :heads], read


def solution(mesh):
    placed = (
        P(None, "sp", None),
        P(),
        P(None, "tp"),
        P(None, "tp"),
        P(None, "tp"),
        P(),
        P(),
        P(),
        P("tp", None, "sp"),
        P("tp", None),
    )
    return jax.shard_map(
        functools.partial(per_device, mesh.shape["sp"], mesh.shape["tp"]),
        mesh=mesh,
        in_specs=placed,
        out_specs=(P("tp", "sp", None), P("tp", "sp"), P(None, "tp"), P()),
        check_vma=False,
    )
```

time: 211 us -> 43.4 us (0.21)
  waiting for transfers between devices: 80.4 us -> 0 us
  blocking collectives: 75.4 us -> 0 us
  Pallas kernels: 0 us -> 33.3 us
  matrix products: 22.7 us -> 0 us
  between operations: 14.2 us -> 0.64 us
  other arithmetic: 5.39 us -> 0 us
  local copies, waits for them, and re-layouts: 12.2 us -> 9.01 us
    reduce_scatter x1 -> x0, waiting for transfers between devices: 69.4 us -> none  [per_device(): lax.psum_scatter(memory_term, 'sp', scatter_dimension=1, tiled=True)]
    all_gather x2 -> x0, blocking collectives: 46.9 us -> none  [the longest x1 27.9 us: per_device(): lax.all_gather(block_total[None], 'sp', axis=0, tiled=True)]
    pallas_call x0 -> x1, Pallas kernels: none -> 33.3 us  [per_device(): pl.pallas_call(functools.partial(kernel, seqs, span, heads, sp, tp), out_...]
    psum x2 -> x0, blocking collectives: 28.4 us -> none  [the longest x1 17.7 us: per_device(): query_state, query_norm = lax.psum((numer_slots, denom_slots), 'sp')]
    dot_general x12 -> x0, matrix products: 22.7 us -> none  [the longest x1 3.63 us: per_device(): jnp.dot(flat, w_value, preferred_element_type=jnp.float32)]
    unnamed x3 -> x0, waiting for transfers between devices: 11 us -> none
    unnamed x14 -> x6, local copies, waits for them, and re-layouts: 3.3 us -> 8.44 us
    convert_element_type x2 -> x0, local copies, waits for them, and re-layouts: 3.1 us -> none  [per_device(): key_heads.astype(jnp.float32) * weight[:, :, :, None]]
  transfers between devices with their start and end apart: 2 -> 0, of which waited for: 2 -> 0; matrix products, arithmetic and copies ran while one was open for 10% -> 0% of each run, Pallas kernels for 0% -> 0%
where the time goes in v1:
time: 43.4 us; the launch traced here: 43 us
  Pallas kernels  33.3 us (77%)
  local copies, waits for them, and re-layouts  9.01 us (21%)
  between operations  0.64 us (1%)
    pallas_call x1, Pallas kernels, per_device(): pl.pallas_call(functools.partial(kernel, seqs, span, heads, sp, tp), out_...  33.3 us
    unnamed x6, local copies, waits for them, and re-layouts  8.44 us

profile of v1, /device:TPU:0, one launch (start us, length us, event | category | flops | bytes accessed | tf_op | source)
XLA Modules:
  0.0 43.0 jit_solution(17333658270431425485)
XLA Ops:
  0.6 1.8 %copy.14.w_in = bf16[2048,8]{1,0:T(8,128)(2,1)} copy(bf16[2048,8]{0,1:T(8,128)(2,1)} %param.15) | data formatting | bytes 65536 | tf_op args[5]
  2.4 1.8 %copy.15.w_forget = bf16[2048,8]{1,0:T(8,128)(2,1)} copy(bf16[2048,8]{0,1:T(8,128)(2,1)} %param.16) | data formatting | bytes 65536 | tf_op args[6]
  4.2 33.3 %shard_map.129 = (bf16[2,128,256]{2,1,0:T(8,128)(2,1)}, f32[2,4,256]{2,1,0:T(4,128)}, f32[4,128]{1,0:T(4,128)}, bf16[4,2048]{1,0:T(4,128)(2,1)}) custom-call(bf16[512,2048]{1,0:T(8,128)(2,1)} %bitcast.5, bf16[4,2048]{1,0:T(4,128)(2,1)} %next_tokens.1, bf16[2048,512]{1,0:T(8,128)(2,1)} %w_query.1, bf16[2048,512]{1,0:T(8,128)(2,1)} %w_key.1, ...), custom_call_target="tpu_custom_call" | custom-call | tf_op jit(solution)/shard_map/pallas_call | solution.py:264
  37.5 0.7 %copy.17 = f32[1,2,4,256]{3,1,2,0:T(2,128)S(1)} copy(f32[1,2,4,256]{3,2,1,0:T(4,128)} %bitcast.7) | data formatting | bytes 16384
  38.2 0.6 %constant_dynamic-slice_fusion = f32[2,128]{1,0:T(2,128)} fusion(f32[2,1024]{1,0:T(2,128)S(1)} %bitcast.6, s32[]{:T(128)S(6)} %select_n.3), kind=kLoop, calls=%fused_computation | loop fusion | bytes 2052 | tf_op jit(solution)/shard_map/dynamic_slice | solution.py:311
  38.7 1.3 %copy.16 = f32[4,2]{0,1:T(2,128)} copy(f32[4,2]{1,0:T(4,128)} %bitcast.8) | data formatting | bytes 64
  40.1 1.6 %copy.20 = bf16[2,128,256]{2,1,0:T(8,128)(2,1)} copy(bf16[2,128,256]{2,1,0:T(8,128)(2,1)} %get-tuple-element.20) | data formatting | bytes 262144
  41.6 1.3 %copy.21 = bf16[4,2048]{1,0:T(4,128)(2,1)} copy(bf16[4,2048]{1,0:T(4,128)(2,1)} %get-tuple-element.23) | data formatting | bytes 32768

commit v2 on v1

--- a/solution.py
+++ b/solution.py
@@ -9,6 +9,7 @@
 
 HD = 256
 LANES = 128
+VMEM_LIMIT = 63 * 1024 * 1024
 F32 = jnp.float32
 BF16 = jnp.bfloat16
 HIGHEST = lax.Precision.HIGHEST
@@ -73,9 +74,9 @@
     x[pl.ds(count, 16), :] = jnp.zeros((16, x.shape[1]), BF16)
     x[pl.ds(count, seqs), :] = next_tokens[...]
     wg[...] = jnp.zeros_like(wg)
-    width = w_in.shape[1]
-    wg[:, 0:width] = w_in[...]
-    wg[:, LANES : LANES + width] = w_forget[...]
+    width = w_in.shape[0]
+    wg[0:width, :] = w_in[...]
+    wg[LANES : LANES + width, :] = w_forget[...]
     bias_wide[...] = jnp.zeros_like(bias_wide)
     bias_wide[0:1, 0:width] = bias[...]
     decay_wide[...] = jnp.zeros_like(decay_wide)
@@ -84,7 +85,7 @@
             decay_wide[p, h : h + 1, :] = decay[h, p : p + 1, :]
 
     load_x.wait()
-    gates = dot(x[...], wg[...])
+    gates = dot(x[...], wg[...], ((1,), (1,)))
     shift = lax.rem(LANES - me_tp * heads, LANES)
     log_in = pltpu.roll(gates[:, :LANES], shift, 1)
     forget = pltpu.roll(log_sigmoid(gates[:, LANES:] + bias_wide[0:1, :]), shift, 1)
@@ -122,7 +123,6 @@
     query = None
     pair_copies = {}
     new_keys, new_values, queries = [], [], []
-    slot_copies = []
 
     for h in range(heads):
         load_k[h].wait()
@@ -148,19 +148,24 @@
             stab = jnp.maximum(stab, later)
             factor = jnp.exp(here - stab)
             stab_out[...] = stab
-        for p in range(seqs):
-            part = slice(p * span, (p + 1) * span)
-            block = dot(weighted[part], values[part], ((0,), (0,)))
-            state[h, pl.ds(p * HD, HD), :] = block * factor[p : p + 1, h : h + 1]
-        for k in order:
-            owner = 2 * lax.rem(group + k, groups) + 1 - side
-            start = pl.multiple_of(owner * rows, rows)
-            pair_send[h, k] = state[h, pl.ds(start, rows), :].astype(BF16)
-            i = h * groups + k
-            pair_copies[h, k] = send(
-                pair_send.at[h, k], pair_recv.at[h, k], pair_ss.at[i], pair_rs.at[i],
-                {"sp": partner},
-            )
+
+        def states():
+            for p in range(seqs):
+                part = slice(p * span, (p + 1) * span)
+                block = dot(weighted[part], values[part], ((0,), (0,)))
+                state[h, pl.ds(p * HD, HD), :] = block * factor[p : p + 1, h : h + 1]
+            for k in order:
+                owner = 2 * lax.rem(group + k, groups) + 1 - side
+                start = pl.multiple_of(owner * rows, rows)
+                pair_send[h, k] = state[h, pl.ds(start, rows), :].astype(BF16)
+                i = h * groups + k
+                pair_copies[h, k] = send(
+                    pair_send.at[h, k], pair_recv.at[h, k], pair_ss.at[i], pair_rs.at[i],
+                    {"sp": partner},
+                )
+
+        if h < heads - 1:
+            states()
         if query is None:
             load_q.wait()
             query = dot(x[pl.ds(count, 16), :], wq[...]).astype(BF16)
@@ -173,11 +178,15 @@
         norm = dot(pick, weighted)
         slots[0, 0, h] = product[:seqs] * factor[:, h : h + 1]
         slots[0, 1, h] = norm[:seqs] * factor[:, h : h + 1]
-
-    slot_copies = [
-        send(slots.at[0], slots.at[k], slot_ss.at[k], slot_rs.at[k], {"sp": lax.rem(me + k, sp)})
-        for k in range(1, sp)
-    ]
+        if h == heads - 1:
+            slot_copies = [
+                send(
+                    slots.at[0], slots.at[k], slot_ss.at[k], slot_rs.at[k],
+                    {"sp": lax.rem(me + k, sp)},
+                )
+                for k in range(1, sp)
+            ]
+            states()
 
     far_copies = {}
 
@@ -213,7 +222,12 @@
     take = jnp.exp(new_in - top)
     outs = []
     for h in range(heads):
-        norm_out[h] = total[1][h]
+        mine_at = lax.broadcasted_iota(jnp.int32, (seqs, HD), 0) == me * rows // HD
+        row = jnp.sum(jnp.where(mine_at, total[1][h], 0.0), axis=0, keepdims=True)
+        turn = lax.rem(HD - lax.rem(me * rows, HD), HD)
+        if rows < HD:
+            row = pltpu.roll(jnp.broadcast_to(row, (8, HD)), turn, 1)[0:1, :rows]
+        norm_out[h : h + 1, :] = row
         keep_h = keep[:, h : h + 1]
         taken = take[:, h : h + 1] * jnp.sum(queries[h] * new_keys[h], axis=1, keepdims=True)
         numer = keep_h * total[0][h] + taken * new_values[h]
@@ -248,6 +262,15 @@
         mem_out[h] = mine.astype(BF16)
 
 
+def finish(memory, norm, stab, read, memory_out, norm_out, stab_out, read_out):
+    memory_out[...] = memory[...]
+    norm_out[...] = norm[...]
+    heads, seqs = stab_out.shape
+    wide = jnp.concatenate([stab[...], jnp.zeros((8 - seqs, LANES), F32)], axis=0)
+    stab_out[...] = wide.T[:heads, :seqs]
+    read_out[...] = read[...]
+
+
 def per_device(
     sp, tp,
     tokens, next_tokens, w_query, w_key, w_value, w_in_gate, w_forget_gate, forget_bias,
@@ -258,14 +281,14 @@
     rows = seqs * HD // sp
     groups = sp // 2
     count = seqs * span
-    any_spec = pl.BlockSpec(memory_space=pl.ANY)
+    any_spec = pl.BlockSpec(memory_space=pltpu.HBM)
     vmem = pl.BlockSpec(memory_space=pltpu.VMEM)
     dma = pltpu.SemaphoreType.DMA
     memory, norm, stab, read = pl.pallas_call(
         functools.partial(kernel, seqs, span, heads, sp, tp),
         out_shape=(
             jax.ShapeDtypeStruct((heads, rows, HD), BF16),
-            jax.ShapeDtypeStruct((heads, seqs, HD), F32),
+            jax.ShapeDtypeStruct((heads, rows), F32),
             jax.ShapeDtypeStruct((seqs, LANES), F32),
             jax.ShapeDtypeStruct((seqs, w_out.shape[1]), BF16),
         ),
@@ -277,7 +300,7 @@
             pltpu.VMEM((heads, model, HD), BF16),
             pltpu.VMEM((heads, model, HD), BF16),
             pltpu.VMEM(w_out.shape, BF16),
-            pltpu.VMEM((model, 2 * LANES), BF16),
+            pltpu.VMEM((2 * LANES, model), BF16),
             pltpu.VMEM((8, LANES), F32),
             pltpu.VMEM((seqs, LANES, span), F32),
             pltpu.VMEM((sp, 2 * seqs, LANES), F32),
@@ -301,15 +324,25 @@
             dma((tp,)),
         ],
         compiler_params=pltpu.CompilerParams(
-            collective_id=0, has_side_effects=True, vmem_limit_bytes=56 * 1024 * 1024
+            collective_id=0, has_side_effects=True, vmem_limit_bytes=VMEM_LIMIT
         ),
     )(
-        tokens.reshape(count, model), next_tokens, w_query, w_key, w_value, w_in_gate,
-        w_forget_gate, forget_bias.reshape(1, -1), extra_decay, w_out,
+        tokens.reshape(count, model), next_tokens, w_query, w_key, w_value, w_in_gate.T,
+        w_forget_gate.T, forget_bias.reshape(1, -1), extra_decay, w_out,
     )
-    start = lax.axis_index("sp") * rows
-    norm_rows = lax.dynamic_slice_in_dim(norm.reshape(heads, seqs * HD), start, rows, 1)
-    return memory, norm_rows, stab[:, :heads], read
+    memory, norm, stab, read = pl.pallas_call(
+        finish,
+        out_shape=(
+            jax.ShapeDtypeStruct(memory.shape, BF16),
+            jax.ShapeDtypeStruct(norm.shape, F32),
+            jax.ShapeDtypeStruct((heads, seqs), F32),
+            jax.ShapeDtypeStruct(read.shape, BF16),
+        ),
+        in_specs=[vmem] * 4,
+        out_specs=(vmem,) * 4,
+        compiler_params=pltpu.CompilerParams(vmem_limit_bytes=VMEM_LIMIT),
+    )(memory, norm, stab, read)
+    return memory, norm, stab.T, read
 
 
 def solution(mesh):

time: 43.4 us -> 33.5 us (0.77)
  local copies, waits for them, and re-layouts: 9.01 us -> 0 us
  Pallas kernels: 33.3 us -> 32.6 us
    unnamed x6 -> x0, local copies, waits for them, and re-layouts: 8.44 us -> none
    pallas_call x1, Pallas kernels: 33.3 us -> 31 us  [per_device(): pl.pallas_call(functools.partial(kernel, seqs, span, heads, sp, tp), out_...]
    pallas_call x0 -> x1, Pallas kernels: none -> 1.58 us  [per_device(): pl.pallas_call(finish, out_shape=(jax.ShapeDtypeStruct(memory.shape, BF16...]
    dynamic_slice x1 -> x0, local copies, waits for them, and re-layouts: 0.56 us -> none  [per_device(): lax.dynamic_slice_in_dim(norm.reshape(heads, seqs * HD), start, rows, 1)]
where the time goes in v2:
time: 33.5 us; the launch traced here: 33.2 us
  Pallas kernels  32.6 us (97%)
  between operations  0.64 us (2%)
    pallas_call x1, Pallas kernels, per_device(): pl.pallas_call(functools.partial(kernel, seqs, span, heads, sp, tp), out_...  31 us
    pallas_call x1, Pallas kernels, per_device(): pl.pallas_call(finish, out_shape=(jax.ShapeDtypeStruct(memory.shape, BF16...  1.58 us

profile of v2, /device:TPU:0, one launch (start us, length us, event | category | flops | bytes accessed | tf_op | source)
XLA Modules:
  0.0 33.2 jit_solution(1559263120857037590)
XLA Ops:
  0.6 31.0 %shard_map.129 = (bf16[2,128,256]{2,1,0:T(8,128)(2,1)}, f32[2,128]{1,0:T(2,128)}, f32[4,128]{1,0:T(4,128)}, bf16[4,2048]{1,0:T(4,128)(2,1)}) custom-call(bf16[512,2048]{1,0:T(8,128)(2,1)} %bitcast.5, bf16[4,2048]{1,0:T(4,128)(2,1)} %next_tokens.1, bf16[2048,512]{1,0:T(8,128)(2,1)} %w_query.1, bf16[2048,512]{1,0:T(8,128)(2,1)} %w_key.1, ...), custom_call_target="tpu_custom_call" | custom-call | tf_op jit(solution)/shard_map/pallas_call | solution.py:287
  31.7 1.6 %shard_map.130 = (bf16[2,128,256]{2,1,0:T(8,128)(2,1)}, f32[2,128]{1,0:T(2,128)}, f32[2,4]{1,0:T(2,128)}, bf16[4,2048]{1,0:T(4,128)(2,1)}) custom-call(bf16[2,128,256]{2,1,0:T(8,128)(2,1)} %get-tuple-element.12.memory, f32[2,128]{1,0:T(2,128)} %get-tuple-element.13.norm, f32[4,128]{1,0:T(4,128)} %get-tuple-element.14.stab, ...), custom_call_target="tpu_custom_call" | custom-call | tf_op jit(solution)/shard_map/pallas_call | solution.py:333

commit v3 on v2

--- a/solution.py
+++ b/solution.py
@@ -41,28 +41,29 @@
     partner = me + 1 - 2 * side
     scale = HD ** (-0.5)
 
-    loads = []
-
-    def load(src, dst):
-        loads.append(pltpu.make_async_copy(src, dst, load_sem.at[len(loads)]))
-        loads[-1].start()
-        return loads[-1]
-
-    load_x = load(tokens, x.at[pl.ds(0, count)])
-    load_k = [None] * heads
-    load_v = [None] * heads
-    for h in range(heads):
-        cols = pl.ds(h * HD, HD)
-        load_k[h] = load(w_key.at[:, cols], wk.at[h])
-        load_v[h] = load(w_value.at[:, cols], wv.at[h])
-    load_q = load(w_query, wq)
-    load_o = load(w_out, wo)
-
     barrier = pltpu.get_barrier_semaphore()
     for k in range(1, sp):
         pl.semaphore_signal(barrier, inc=1, device_id={"sp": lax.rem(me + k, sp)})
     for k in range(1, tp):
         pl.semaphore_signal(barrier, inc=1, device_id={"tp": lax.rem(me_tp + k, tp)})
+
+    loads = []
+
+    def load(src, dst):
+        loads.append(pltpu.make_async_copy(src, dst, load_sem.at[len(loads)]))
+        loads[-1].start()
+        return loads[-1]
+
+    load_x = load(tokens, x.at[pl.ds(0, count)])
+    load_k = [None] * heads
+    load_v = [None] * heads
+
+    def load_head(h):
+        cols = pl.ds(h * HD, HD)
+        load_k[h] = load(w_key.at[:, cols], wk.at[h])
+        load_v[h] = load(w_value.at[:, cols], wv.at[h])
+
+    load_head(0)
 
     def send(src, dst, ss, rs, where):
         copy = pltpu.make_async_remote_copy(
@@ -85,6 +86,10 @@
             decay_wide[p, h : h + 1, :] = decay[h, p : p + 1, :]
 
     load_x.wait()
+    for h in range(1, heads):
+        load_head(h)
+    load_q = load(w_query, wq)
+    load_o = load(w_out, wo)
     gates = dot(x[...], wg[...], ((1,), (1,)))
     shift = lax.rem(LANES - me_tp * heads, LANES)
     log_in = pltpu.roll(gates[:, :LANES], shift, 1)
@@ -119,10 +124,9 @@
         == lax.broadcasted_iota(jnp.int32, (16, count), 0)
     )
     pick = jnp.where(mask, 1.0, 0.0).astype(BF16)
-    factor = None
     query = None
     pair_copies = {}
-    new_keys, new_values, queries = [], [], []
+    new_keys, new_values, queries, products, norms = [], [], [], [], []
 
     for h in range(heads):
         load_k[h].wait()
@@ -132,28 +136,12 @@
         weighted = (keys[:count].astype(F32) * weight[:, h : h + 1]).astype(BF16)
         new_keys.append(keys[count : count + seqs].astype(F32) * scale)
         new_values.append(values[count : count + seqs].astype(F32))
-        if factor is None:
-            for copy in stat_copies:
-                copy.wait()
-            later = jnp.zeros((seqs, LANES), F32)
-            stab = None
-            here = later
-            for s in range(sp - 1, -1, -1):
-                slot = lax.rem(me - s + sp, sp)
-                peak = stats[slot, seqs : 2 * seqs, :]
-                total = stats[slot, 0:seqs, :]
-                stab = later + peak if stab is None else jnp.maximum(stab, later + peak)
-                here = jnp.where(me == s, later + peak, here)
-                later = later + total
-            stab = jnp.maximum(stab, later)
-            factor = jnp.exp(here - stab)
-            stab_out[...] = stab
 
         def states():
             for p in range(seqs):
                 part = slice(p * span, (p + 1) * span)
                 block = dot(weighted[part], values[part], ((0,), (0,)))
-                state[h, pl.ds(p * HD, HD), :] = block * factor[p : p + 1, h : h + 1]
+                state[h, pl.ds(p * HD, HD), :] = block
             for k in order:
                 owner = 2 * lax.rem(group + k, groups) + 1 - side
                 start = pl.multiple_of(owner * rows, rows)
@@ -176,9 +164,27 @@
         low = (reach - high.astype(F32)).astype(BF16)
         product = dot(high, values[:count]) + dot(low, values[:count])
         norm = dot(pick, weighted)
-        slots[0, 0, h] = product[:seqs] * factor[:, h : h + 1]
-        slots[0, 1, h] = norm[:seqs] * factor[:, h : h + 1]
+        products.append(product[:seqs])
+        norms.append(norm[:seqs])
         if h == heads - 1:
+            for copy in stat_copies:
+                copy.wait()
+            later = jnp.zeros((seqs, LANES), F32)
+            stab, here, there = None, later, later
+            for s in range(sp - 1, -1, -1):
+                slot = lax.rem(me - s + sp, sp)
+                level = later + stats[slot, seqs : 2 * seqs, :]
+                stab = level if stab is None else jnp.maximum(stab, level)
+                here = jnp.where(me == s, level, here)
+                there = jnp.where(partner == s, level, there)
+                later = later + stats[slot, 0:seqs, :]
+            stab = jnp.maximum(stab, later)
+            factor = jnp.exp(here - stab)
+            factor_there = jnp.exp(there - stab)
+            stab_out[...] = stab
+            for i in range(heads):
+                slots[0, 0, i] = products[i] * factor[:, i : i + 1]
+                slots[0, 1, i] = norms[i] * factor[:, i : i + 1]
             slot_copies = [
                 send(
                     slots.at[0], slots.at[k], slot_ss.at[k], slot_rs.at[k],
@@ -189,6 +195,14 @@
             states()
 
     far_copies = {}
+    prompt = lax.broadcasted_iota(jnp.int32, (seqs, LANES), 0)
+
+    def pair_sum(h, k, owner):
+        at = prompt == owner * rows // HD
+        mine = jnp.sum(jnp.where(at, factor, 0.0), axis=0, keepdims=True)[:, h : h + 1]
+        other = jnp.sum(jnp.where(at, factor_there, 0.0), axis=0, keepdims=True)[:, h : h + 1]
+        start = pl.multiple_of(owner * rows, rows)
+        return state[h, pl.ds(start, rows), :] * mine + pair_recv[h, k].astype(F32) * other
 
     def forward(h):
         for k in order:
@@ -196,10 +210,7 @@
             if k == 0:
                 continue
             to = lax.rem(group + k, groups)
-            start = pl.multiple_of((2 * to + side) * rows, rows)
-            far_send[h, k] = (
-                state[h, pl.ds(start, rows), :] + pair_recv[h, k].astype(F32)
-            ).astype(BF16)
+            far_send[h, k] = pair_sum(h, k, 2 * to + side).astype(BF16)
             i = h * groups + k
             far_copies[h, k] = send(
                 far_send.at[h, k], far_recv.at[h, k], far_ss.at[i], far_rs.at[i],
@@ -253,9 +264,8 @@
         read = term if read is None else read + term
     read_out[...] = read.astype(BF16)
 
-    start = pl.multiple_of(me * rows, rows)
     for h in range(heads):
-        mine = state[h, pl.ds(start, rows), :] + pair_recv[h, 0].astype(F32)
+        mine = pair_sum(h, 0, me)
         for k in order[:-1]:
             far_copies[h, k].wait()
             mine = mine + far_recv[h, k].astype(F32)

time: 33.5 us -> 32.8 us (0.979)
  Pallas kernels: 32.6 us -> 31.9 us
    pallas_call x1, Pallas kernels: 31 us -> 30.3 us  [per_device(): pl.pallas_call(functools.partial(kernel, seqs, span, heads, sp, tp), out_...]
where the time goes in v3:
time: 32.8 us; the launch traced here: 32.6 us
  Pallas kernels  31.9 us (97%)
  between operations  0.64 us (2%)
    pallas_call x1, Pallas kernels, per_device(): pl.pallas_call(functools.partial(kernel, seqs, span, heads, sp, tp), out_...  30.3 us
    pallas_call x1, Pallas kernels, per_device(): pl.pallas_call(finish, out_shape=(jax.ShapeDtypeStruct(memory.shape, BF16...  1.58 us

profile of v3, /device:TPU:0, one launch (start us, length us, event | category | flops | bytes accessed | tf_op | source)
XLA Modules:
  0.0 32.6 jit_solution(16502418392333865446)
XLA Ops:
  0.6 30.3 %shard_map.129 = (bf16[2,128,256]{2,1,0:T(8,128)(2,1)}, f32[2,128]{1,0:T(2,128)}, f32[4,128]{1,0:T(4,128)}, bf16[4,2048]{1,0:T(4,128)(2,1)}) custom-call(bf16[512,2048]{1,0:T(8,128)(2,1)} %bitcast.5, bf16[4,2048]{1,0:T(4,128)(2,1)} %next_tokens.1, bf16[2048,512]{1,0:T(8,128)(2,1)} %w_query.1, bf16[2048,512]{1,0:T(8,128)(2,1)} %w_key.1, ...), custom_call_target="tpu_custom_call" | custom-call | tf_op jit(solution)/shard_map/pallas_call | solution.py:297
  31.0 1.6 %shard_map.130 = (bf16[2,128,256]{2,1,0:T(8,128)(2,1)}, f32[2,128]{1,0:T(2,128)}, f32[2,4]{1,0:T(2,128)}, bf16[4,2048]{1,0:T(4,128)(2,1)}) custom-call(bf16[2,128,256]{2,1,0:T(8,128)(2,1)} %get-tuple-element.12.memory, f32[2,128]{1,0:T(2,128)} %get-tuple-element.13.norm, f32[4,128]{1,0:T(4,128)} %get-tuple-element.14.stab, ...), custom_call_target="tpu_custom_call" | custom-call | tf_op jit(solution)/shard_map/pallas_call | solution.py:343
